TPU v7x, 32 devices: a whole 2x2x4 slice. The times are simulated.
32 devices in a mesh: sp: 8 (over z, x), tp: 4 (over y, core).
Axes of the slice: x: 2, y: 2, z: 4, core: 2. Of those that a mesh axis runs over, the one named last changes fastest.
Arguments:
- residual_in: bfloat16 [2048, 2048], P(('sp', 'tp')), may hold values from -0.119628906 to 0.119628906
- queries: bfloat16 [2048, 2048], P('sp', 'tp'), may hold values from -6 to 6
- keys_raw: bfloat16 [2048, 512], P('sp', 'tp'), may hold values from -6 to 6
- values_raw: bfloat16 [2048, 512], P('sp', 'tp'), may hold values from -6 to 6
- query_gain: float32 [128], replicated, may hold values from 0.28 to 7
- key_gain: float32 [128], replicated, may hold values from 0.28 to 7
- out_weight: bfloat16 [2048, 2048], P('tp'), may hold values from -0.125 to 0.125
- norm_gain: float32 [2048], replicated, may hold values from 0.1 to 1.9
- gate_weight: bfloat16 [2048, 5632], P('sp', 'tp'), may hold values from -0.125 to 0.125
- up_weight: bfloat16 [2048, 5632], P('sp', 'tp'), may hold values from -0.125 to 0.125
- down_weight: bfloat16 [5632, 2048], P('tp', 'sp'), may hold values from -0.078125 to 0.078125
Outputs:
- residual_out: bfloat16 [2048, 2048], P(('sp', 'tp'))
All inputs are finite; a program needn't handle non-finite values.
Results may differ from a plain program's by a relative error of at most 0.024.
The roundings to bfloat16 on the way count: a program that leaves them out, or rounds other values in their place, can miss the bound.
Values may be sent and summed in bfloat16 or wider, within the bound.
A program may use at most 128 MiB of HBM per device.

v0:
```python
import jax
import jax.numpy as jnp
from jax import lax
from jax.sharding import PartitionSpec as P

GRID_W = 64
EPS = 1e-06
THETA = 10000.0


def turn_half(part, angles):
    quarter = part.shape[-1] // 2
    cosine = jnp.cos(angles)[:, None, :]
    sine = jnp.sin(angles)[:, None, :]
    first = part[..., :quarter]
    second = part[..., quarter:]
    return part * cosine + jnp.concatenate([-second, first], axis=-1) * sine


def prepare_heads(raw, gain, positions, heads):
    count = raw.shape[0]
    head_dim = gain.shape[0]
    half = head_dim // 2
    vec = raw.astype(jnp.float32).reshape(count, heads, head_dim)
    vec = vec * lax.rsqrt(jnp.mean(vec * vec, axis=-1, keepdims=True) + EPS) * gain
    freqs = THETA ** (-jnp.arange(0, half, 2, dtype=jnp.float32) / half)
    row_ang = (positions // GRID_W).astype(jnp.float32)[:, None] * freqs
    col_ang = (positions % GRID_W).astype(jnp.float32)[:, None] * freqs
    row_ang = jnp.concatenate([row_ang, row_ang], axis=-1)
    col_ang = jnp.concatenate([col_ang, col_ang], axis=-1)
    turned = jnp.concatenate(
        [turn_half(vec[..., :half], row_ang), turn_half(vec[..., half:], col_ang)], axis=-1
    )
    return turned.astype(jnp.bfloat16)


def per_device(
    residual_in,
    queries,
    keys_raw,
    values_raw,
    query_gain,
    key_gain,
    out_weight,
    norm_gain,
    gate_weight,
    up_weight,
    down_weight,
):
    tok = queries.shape[0]
    head_dim = query_gain.shape[0]
    local_heads = queries.shape[1] // head_dim
    local_kv = keys_raw.shape[1] // head_dim
    group = local_heads // local_kv
    gate_full, up_full = (
        lax.all_gather(gate_weight, "sp", axis=0, tiled=True),
        lax.all_gather(up_weight, "sp", axis=0, tiled=True),
    )
    down_full = lax.all_gather(down_weight, "sp", axis=1, tiled=True)
    positions = lax.axis_index("sp") * tok + jnp.arange(tok, dtype=jnp.int32)
    q_rot = prepare_heads(queries, query_gain, positions, local_heads).reshape(
        tok, local_kv, group, head_dim
    )
    k_rot = prepare_heads(keys_raw, key_gain, positions, local_kv)
    vals = values_raw.reshape(tok, local_kv, head_dim)
    start_state = (
        jnp.full((tok, local_kv, group), -jnp.inf, jnp.float32),
        jnp.zeros((tok, local_kv, group), jnp.float32),
        jnp.zeros((tok, local_kv, group, head_dim), jnp.float32),
    )
    carry = start_state
    k_piece = lax.all_gather(k_rot, "sp", axis=0, tiled=True)
    v_piece = lax.all_gather(vals, "sp", axis=0, tiled=True)
    length = k_piece.shape[0]
    shards = length // tok
    per_step = max(1, 2048 // tok)
    factor = max((d for d in range(1, shards + 1) if shards % d == 0 and d <= per_step))
    span = factor * tok
    k_blocks = k_piece.reshape(length // span, span, local_kv, head_dim)
    v_blocks = v_piece.reshape(length // span, span, local_kv, head_dim)

    def step(state, blocks):
        top, total, summed = state
        k_blk, v_blk = blocks
        scores = jnp.einsum(
            "qkgd,skd->qkgs", q_rot, k_blk, preferred_element_type=jnp.float32
        ) * head_dim ** (-0.5)
        new_top = jnp.maximum(top, jnp.max(scores, axis=-1))
        shrink = jnp.exp(top - new_top)
        expo = jnp.exp(scores - new_top[..., None])
        total = total * shrink + jnp.sum(expo, axis=-1)
        summed = summed * shrink[..., None] + jnp.einsum(
            "qkgs,skd->qkgd", expo.astype(jnp.bfloat16), v_blk, preferred_element_type=jnp.float32
        )
        return ((new_top, total, summed), None)

    carry, _ = lax.scan(step, carry, (k_blocks, v_blocks))
    top, total, summed = carry
    attended = (summed / total[..., None]).astype(jnp.bfloat16).reshape(tok, local_heads * head_dim)
    projected = lax.psum_scatter(
        jnp.dot(attended, out_weight, preferred_element_type=jnp.float32).astype(jnp.bfloat16),
        "tp",
        scatter_dimension=0,
        tiled=True,
    ).astype(jnp.float32)
    mixed = (residual_in.astype(jnp.float32) + projected).astype(jnp.bfloat16)
    mixed_f = mixed.astype(jnp.float32)
    normed = (
        mixed_f * lax.rsqrt(jnp.mean(mixed_f * mixed_f, axis=-1, keepdims=True) + EPS) * norm_gain
    ).astype(jnp.bfloat16)
    whole_rows = lax.all_gather(normed, "tp", axis=0, tiled=True)
    gate = jnp.dot(whole_rows, gate_full, preferred_element_type=jnp.float32)
    up_val = jnp.dot(whole_rows, up_full, preferred_element_type=jnp.float32)
    hidden = (jax.nn.silu(gate) * up_val).astype(jnp.bfloat16)
    terms = jnp.dot(hidden, down_full, preferred_element_type=jnp.float32)
    fed = lax.psum_scatter(
        terms.astype(jnp.bfloat16), "tp", scatter_dimension=0, tiled=True
    ).astype(jnp.float32)
    return (mixed_f + 0.5 * fed).astype(jnp.bfloat16)


def solution(mesh):
    placed = (
        P(("sp", "tp"), None),
        P("sp", "tp"),
        P("sp", "tp"),
        P("sp", "tp"),
        P(),
        P(),
        P("tp", None),
        P(),
        P("sp", "tp"),
        P("sp", "tp"),
        P("tp", "sp"),
    )
    return jax.shard_map(
        per_device, mesh=mesh, in_specs=placed, out_specs=P(("sp", "tp"), None), check_vma=False
    )
```

profile of v0, /device:TPU:0, one launch (start us, length us, event | category | flops | bytes accessed | tf_op | source)
XLA Modules:
  0.0 460.9 jit_solution(13443270139341550448)
XLA Ops:
  6.6 1.1 fusion.33
  7.7 0.9 fusion.35
  9.6 1.2 fusion.39
  10.9 33.0 %all_gather.18 = bf16[2048,1,128]{2,0,1:T(8,128)(2,1)S(1)} all-gather(bf16[256,1,128]{2,0,1:T(8,128)(2,1)S(1)} %pad_maximum_fusion.4), channel_id=1, replica_groups=mesh['sp'=8,'tp'=4] {'sp'}, dimensions={0}, use_global_device_ids=true | all-gather | bytes 589824 | tf_op jit(solution)/shard_map/all_gather | solution.py:72
  43.9 1.1 copy.14
  45.2 0.9 multiply_multiply_fusion
  46.6 1.5 fusion.43
  49.1 1.3 bitcast_reduce_fusion
  50.5 3.2 copy-done.1
  53.7 1.4 fusion.1
  55.2 31.3 %all-gather = bf16[2048,128]{0,1:T(8,128)(2,1)S(1)} all-gather(bf16[256,128]{0,1:T(8,128)(2,1)S(1)} %copy.16), channel_id=2, replica_groups=mesh['sp'=8,'tp'=4] {'sp'}, dimensions={0}, use_global_device_ids=true | all-gather | bytes 589824 | tf_op jit(solution)/shard_map/all_gather | solution.py:73
  86.5 5.1 %fusion.16 = bf16[1,128,256,4]{2,1,3,0:T(8,128)(2,1)S(1)} fusion(f32[2048,256,4]{1,0,2:T(8,128)} %copy-done.1, f32[256,4]{0,1:T(4,128)S(1)} %get-tuple-element.50, bf16[2048,128]{0,1:T(8,128)(2,1)S(1)} %all-gather, f32[256,4]{0,1:T(4,128)S(1)} %get-tuple-element.43, f32[256,4]{0,1:T(4,128)S(1)} %get-tuple-element.42), kind=kOutput, calls=%fused_computation.14 | convolution fusion | flops 543555584 | bytes 9187328 | tf_op jit(solution)/shard_map/while/body/eval_jaxpr/qkgs,skd->qkgd/dot_general | solution.py:92
  91.6 1.7 convolution_convert_fusion
  93.4 26.1 %reduce-scatter.3.cloned.1.call-done = bf16[64,2048]{1,0:T(8,128)(2,1)} async-done(((bf16[256,2048]{1,0:T(8,128)(2,1)}), bf16[64,2048]{1,0:T(8,128)(2,1)}) %reduce-scatter.3.cloned.1.call-update) | async-done | bytes 262160 | tf_op jit(solution)/shard_map/reduce_scatter | solution.py:100
  119.4 1.1 fusion.19
  120.6 1.8 fusion.21
  124.5 14.7 %all-gather.6.cloned.1.call-done = bf16[256,2048]{1,0:T(8,128)(2,1)} async-done(((bf16[64,2048]{1,0:T(8,128)(2,1)}), bf16[256,2048]{1,0:T(8,128)(2,1)}) %all-gather.6.cloned.1.call-update) | async-done | bytes 1048592 | tf_op jit(solution)/shard_map/all_gather | solution.py:111
  139.3 94.5 %all-gather.8.cloned.1.call-done = bf16[2048,1408]{1,0:T(8,128)(2,1)} async-done(((bf16[256,1408]{1,0:T(8,128)(2,1)}), bf16[2048,1408]{1,0:T(8,128)(2,1)}) %all-gather.8.cloned.1.call-update) | async-done | bytes 5767184 | tf_op jit(solution)/shard_map/all_gather | solution.py:56
  233.8 5.9 %fusion.53 = f32[256,1408]{1,0:T(8,128)} fusion(bf16[256,2048]{1,0:T(8,128)(2,1)} %all-gather.6.cloned.1.call-done, bf16[2048,1408]{1,0:T(8,128)(2,1)} %all-gather.8.cloned.1.call-done), kind=kOutput, calls=%fused_computation.88 | convolution fusion | flops 1476395008 | bytes 8257536 | tf_op jit(solution)/shard_map/dot_general | solution.py:112
  239.7 86.7 %all-gather.10.cloned.1.call-done = bf16[2048,1408]{1,0:T(8,128)(2,1)} async-done(((bf16[256,1408]{1,0:T(8,128)(2,1)}), bf16[2048,1408]{1,0:T(8,128)(2,1)}) %all-gather.10.cloned.1.call-update) | async-done | bytes 5767184 | tf_op jit(solution)/shard_map/all_gather | solution.py:57
  326.3 93.2 %all-gather.12.cloned.1.call-done = bf16[1408,2048]{1,0:T(8,128)(2,1)} async-done(((bf16[1408,256]{1,0:T(8,128)(2,1)}), bf16[1408,2048]{1,0:T(8,128)(2,1)}) %all-gather.12.cloned.1.call-update) | async-done | bytes 5767184 | tf_op jit(solution)/shard_map/all_gather | solution.py:59
  419.6 9.5 %convolution_convert_fusion.1 = bf16[256,2048]{1,0:T(8,128)(2,1)} fusion(bf16[1408,2048]{1,0:T(8,128)(2,1)} %all-gather.12.cloned.1.call-done, bf16[256,2048]{1,0:T(8,128)(2,1)} %all-gather.6.cloned.1.call-done, bf16[2048,1408]{1,0:T(8,128)(2,1)} %all-gather.10.cloned.1.call-done, f32[256,1408]{1,0:T(8,128)} %fusion.53), kind=kOutput, calls=%fused_computation.10 | convolution fusion | flops 2955476992 | bytes 15073280 | tf_op jit(solution)/shard_map/dot_general | solution.py:115
  429.1 23.1 %reduce-scatter.5.cloned.1.call-done = bf16[64,2048]{1,0:T(8,128)(2,1)} async-done(((bf16[256,2048]{1,0:T(8,128)(2,1)}), bf16[64,2048]{1,0:T(8,128)(2,1)}) %reduce-scatter.5.cloned.1.call-update) | async-done | bytes 262160 | tf_op jit(solution)/shard_map/reduce_scatter | solution.py:116
  452.3 1.8 fusion.22
  (38 shorter events, 5.1 us)
Async XLA Ops:
  6.5 85.0 %copy-start = (bf16[512,2048]{1,0:T(8,128)(2,1)S(1)}, bf16[512,2048]{1,0:T(8,128)(2,1)}, u32[]{:S(2)}) copy-start(bf16[512,2048]{1,0:T(8,128)(2,1)} %param.17) | copy-start | bytes 6291460
  6.5 112.9 %reduce-scatter.3.cloned.1.call-start = ((), (), s32[]{:S(2)}) async-start(), calls=%async_computation.2 | async-start | bytes 1310720 | tf_op jit(solution)/shard_map/reduce_scatter | solution.py:100
  50.5 3.2 copy-start.1
  50.5 4.6 %copy-start.4 = (bf16[256,128]{1,0:T(8,128)(2,1)S(1)}, bf16[256,128]{1,0:T(8,128)(2,1)}, u32[]{:S(2)}) copy-start(bf16[256,128]{1,0:T(8,128)(2,1)} %param.14) | copy-start | bytes 196612
  86.5 32.9 %copy-start.2 = (bf16[64,2048]{1,0:T(8,128)(2,1)S(1)}, bf16[64,2048]{1,0:T(8,128)(2,1)}, u32[]{:S(2)}) copy-start(bf16[64,2048]{1,0:T(8,128)(2,1)} %param.11) | copy-start | bytes 786436
  86.5 34.1 %copy-start.5 = (f32[2048]{0:T(1024)S(1)}, f32[2048]{0:T(1024)}, u32[]{:S(2)}) copy-start(f32[2048]{0:T(1024)} %param.18) | copy-start | bytes 24580
  93.3 45.9 %all-gather.6.cloned.1.call-start = ((), (), s32[]{:S(2)}) async-start(), calls=%async_computation.3 | async-start | bytes 1310720 | tf_op jit(solution)/shard_map/all_gather | solution.py:111
  122.4 111.4 %all-gather.8.cloned.1.call-start = ((), (), s32[]{:S(2)}) async-start(), calls=%async_computation.4 | async-start | bytes 6488064 | tf_op jit(solution)/shard_map/all_gather | solution.py:56
  123.1 203.2 %all-gather.10.cloned.1.call-start = ((), (), s32[]{:S(2)}) async-start(), calls=%async_computation.5 | async-start | bytes 6488064 | tf_op jit(solution)/shard_map/all_gather | solution.py:57
  123.7 295.9 %all-gather.12.cloned.1.call-start = ((), (), s32[]{:S(2)}) async-start(), calls=%async_computation.6 | async-start | bytes 6488064 | tf_op jit(solution)/shard_map/all_gather | solution.py:59
  124.3 327.9 %reduce-scatter.5.cloned.1.call-start = ((), (), s32[]{:S(2)}) async-start(), calls=%async_computation.7 | async-start | bytes 1310720 | tf_op jit(solution)/shard_map/reduce_scatter | solution.py:116
  239.7 212.6 %copy-start.3 = (bf16[64,2048]{1,0:T(8,128)(2,1)S(1)}, bf16[64,2048]{1,0:T(8,128)(2,1)}, u32[]{:S(2)}) copy-start(bf16[64,2048]{1,0:T(8,128)(2,1)} %reduce-scatter.3.cloned.1.call-done) | copy-start | bytes 786436
Sparse Core Ops, SparseCore 0:
  93.4 25.9 reduce-scatter.2
  122.5 16.6 all-gather.5
  141.4 92.2 all-gather.7
  235.8 90.4 all-gather.9
  328.2 91.2 all-gather.11
  429.2 22.9 reduce-scatter.4
where the time goes:
time: 461 us
  waiting for transfers between devices  340 us (74%)
  blocking collectives  64.3 us (14%)
  matrix products  23.5 us (5%)
  other arithmetic  14.3 us (3%)
  between operations  13.6 us (3%)
    all_gather x1, waiting for transfers between devices, per_device(): lax.all_gather(gate_weight, 'sp', axis=0, tiled=True)  94.5 us
    all_gather x1, waiting for transfers between devices, per_device(): down_full = lax.all_gather(down_weight, 'sp', axis=1, tiled=True)  93.2 us
    all_gather x1, waiting for transfers between devices, per_device(): lax.all_gather(up_weight, 'sp', axis=0, tiled=True)  86.7 us
    all_gather x1, blocking collectives, per_device(): k_piece = lax.all_gather(k_rot, 'sp', axis=0, tiled=True)  33 us
    all_gather x1, blocking collectives, per_device(): v_piece = lax.all_gather(vals, 'sp', axis=0, tiled=True)  31.3 us
    reduce_scatter x1, waiting for transfers between devices, per_device(): lax.psum_scatter(jnp.dot(attended, out_weight, preferred_element_type=jnp...  26.1 us
    reduce_scatter x1, waiting for transfers between devices, per_device(): lax.psum_scatter(terms.astype(jnp.bfloat16), 'tp', scatter_dimension=0, t...  23.1 us
    all_gather x1, waiting for transfers between devices, per_device(): whole_rows = lax.all_gather(normed, 'tp', axis=0, tiled=True)  14.7 us
  transfers between devices with their start and end apart: 6, of which 6 were waited for; matrix products, arithmetic and copies ran while one was open for 1% of the time, Pallas kernels for 0%

commit v1 on v0

--- a/solution.py
+++ b/solution.py
@@ -70,7 +70,12 @@
     )
     carry = start_state
     k_piece = lax.all_gather(k_rot, "sp", axis=0, tiled=True)
-    v_piece = lax.all_gather(vals, "sp", axis=0, tiled=True)
+    ring = [vals]
+    for hop in range(7):
+        ring.append(lax.ppermute(ring[-1], "sp", [(dev, (dev + 1) % 8) for dev in range(8)]))
+    v_piece = jnp.roll(
+        jnp.concatenate(ring[::-1], axis=0), (lax.axis_index("sp") + 1) * ring[0].shape[0], axis=0
+    )
     length = k_piece.shape[0]
     shards = length // tok
     per_step = max(1, 2048 // tok)

time: 461 us -> 457 us (level)
  blocking collectives: 64.3 us -> 31.5 us
  waiting for transfers between devices: 340 us -> 364 us
  starting transfers between devices: 0.38 us -> 6.83 us
    all_gather x1 -> x0, blocking collectives: 31.3 us -> none  [per_device(): v_piece = lax.all_gather(vals, 'sp', axis=0, tiled=True)]
    ppermute x0 -> x7, waiting for transfers between devices: none -> 27.5 us  [per_device(): lax.ppermute(ring[-1], 'sp', [(dev, (dev + 1) % 8) for dev in range(8)])]
    ppermute x0 -> x7, starting transfers between devices: none -> 6.45 us  [per_device(): lax.ppermute(ring[-1], 'sp', [(dev, (dev + 1) % 8) for dev in range(8)])]
    all_gather x1, waiting for transfers between devices: 86.7 us -> 92.6 us  [per_device(): lax.all_gather(up_weight, 'sp', axis=0, tiled=True)]
    all_gather x1, waiting for transfers between devices: 93.2 us -> 87.3 us  [per_device(): down_full = lax.all_gather(down_weight, 'sp', axis=1, tiled=True)]
  transfers between devices with their start and end apart: 6 -> 13, of which waited for: 6 -> 11; matrix products, arithmetic and copies ran while one was open for 1% -> 4% of each run, Pallas kernels for 0% -> 0%
where the time goes in v1:
time: 457 us
  waiting for transfers between devices  364 us (80%)
  blocking collectives  31.5 us (7%)
  matrix products  23.6 us (5%)
  other arithmetic  14.1 us (3%)
  between operations  13.7 us (3%)
  starting transfers between devices  6.83 us (1%)
    all_gather x1, waiting for transfers between devices, per_device(): lax.all_gather(gate_weight, 'sp', axis=0, tiled=True)  94.5 us
    all_gather x1, waiting for transfers between devices, per_device(): lax.all_gather(up_weight, 'sp', axis=0, tiled=True)  92.6 us
    all_gather x1, waiting for transfers between devices, per_device(): down_full = lax.all_gather(down_weight, 'sp', axis=1, tiled=True)  87.3 us
    all_gather x1, blocking collectives, per_device(): k_piece = lax.all_gather(k_rot, 'sp', axis=0, tiled=True)  31.5 us
    ppermute x7, waiting for transfers between devices, per_device(): lax.ppermute(ring[-1], 'sp', [(dev, (dev + 1) % 8) for dev in range(8)])  27.5 us
    reduce_scatter x1, waiting for transfers between devices, per_device(): lax.psum_scatter(terms.astype(jnp.bfloat16), 'tp', scatter_dimension=0, t...  23.2 us
    reduce_scatter x1, waiting for transfers between devices, per_device(): lax.psum_scatter(jnp.dot(attended, out_weight, preferred_element_type=jnp...  22.2 us
    all_gather x1, waiting for transfers between devices, per_device(): whole_rows = lax.all_gather(normed, 'tp', axis=0, tiled=True)  14.7 us
  transfers between devices with their start and end apart: 13, of which 11 were waited for; matrix products, arithmetic and copies ran while one was open for 4% of the time, Pallas kernels for 0%

profile of v1, /device:TPU:0, one launch (start us, length us, event | category | flops | bytes accessed | tf_op | source)
XLA Modules:
  0.0 456.7 jit_solution(4861307536852972098)
XLA Ops:
  6.5 3.0 collective-permute-start
  16.0 1.4 fusion.26
  17.6 1.6 collective-permute-start.1
  20.4 4.4 collective-permute-done.1
  24.9 6.9 %collective-permute-done.2 = bf16[256,1,128]{2,0,1:T(8,128)(2,1)S(1)} collective-permute-done((bf16[256,1,128]{2,0,1:T(8,128)(2,1)S(1)}, bf16[256,1,128]{2,0,1:T(8,128)(2,1)S(1)}, u32[]{:S(2)}, u32[]{:S(2)}) %collective-permute-start.2) | collective-permute-done | bytes 65568 | tf_op jit(solution)/shard_map/ppermute | solution.py:75
  31.8 31.5 %all_gather.15 = bf16[2048,1,128]{2,0,1:T(8,128)(2,1)S(1)} all-gather(bf16[256,1,128]{2,0,1:T(8,128)(2,1)S(1)} %pad_maximum_fusion.4), channel_id=1, replica_groups=mesh['sp'=8,'tp'=4] {'sp'}, dimensions={0}, use_global_device_ids=true | all-gather | bytes 589824 | tf_op jit(solution)/shard_map/all_gather | solution.py:72
  63.3 1.9 collective-permute-start.4
  65.2 1.3 bitcast_reduce_fusion
  66.5 3.7 collective-permute-done.4
  70.2 1.4 fusion.1
  71.6 5.6 %collective-permute-done.5 = bf16[256,1,128]{2,0,1:T(8,128)(2,1)S(1)} collective-permute-done((bf16[256,1,128]{2,0,1:T(8,128)(2,1)S(1)}, bf16[256,1,128]{2,0,1:T(8,128)(2,1)S(1)}, u32[]{:S(2)}, u32[]{:S(2)}) %collective-permute-start.5) | collective-permute-done | bytes 65568 | tf_op jit(solution)/shard_map/ppermute | solution.py:75
  77.2 6.9 %collective-permute-done.6 = bf16[256,1,128]{2,0,1:T(8,128)(2,1)S(1)} collective-permute-done((bf16[256,1,128]{2,0,1:T(8,128)(2,1)S(1)}, bf16[256,1,128]{2,0,1:T(8,128)(2,1)S(1)}, u32[]{:S(2)}, u32[]{:S(2)}) %collective-permute-start.6) | collective-permute-done | bytes 65568 | tf_op jit(solution)/shard_map/ppermute | solution.py:75
  86.2 5.1 %fusion.16 = bf16[1,128,256,4]{2,1,3,0:T(8,128)(2,1)S(1)} fusion(f32[2048,256,4]{1,0,2:T(8,128)} %copy-done.1, f32[256,4]{0,1:T(4,128)S(1)} %get-tuple-element.50, bf16[4096,1,128]{2,0,1:T(8,128)(2,1)S(1)} %constant_dynamic-update-slice_fusion, s32[]{:T(128)S(6)} %select_n.38, f32[256,4]{0,1:T(4,128)S(1)} %get-tuple-element.43, ...), kind=kOutput, calls=%fused_computation.14 | convolution fusion | flops 543555584 | bytes 9187332 | tf_op jit(solution)/shard_map/while/body/eval_jaxpr/qkgs,skd->qkgd/dot_general | solution.py:97
  91.3 1.7 convolution_convert_fusion
  93.1 22.2 %reduce-scatter.3.cloned.1.call-done = bf16[64,2048]{1,0:T(8,128)(2,1)} async-done(((bf16[256,2048]{1,0:T(8,128)(2,1)}), bf16[64,2048]{1,0:T(8,128)(2,1)}) %reduce-scatter.3.cloned.1.call-update) | async-done | bytes 262160 | tf_op jit(solution)/shard_map/reduce_scatter | solution.py:105
  116.5 1.8 fusion.21
  120.4 14.7 %all-gather.5.cloned.1.call-done = bf16[256,2048]{1,0:T(8,128)(2,1)} async-done(((bf16[64,2048]{1,0:T(8,128)(2,1)}), bf16[256,2048]{1,0:T(8,128)(2,1)}) %all-gather.5.cloned.1.call-update) | async-done | bytes 1048592 | tf_op jit(solution)/shard_map/all_gather | solution.py:116
  135.1 94.5 %all-gather.7.cloned.1.call-done = bf16[2048,1408]{1,0:T(8,128)(2,1)} async-done(((bf16[256,1408]{1,0:T(8,128)(2,1)}), bf16[2048,1408]{1,0:T(8,128)(2,1)}) %all-gather.7.cloned.1.call-update) | async-done | bytes 5767184 | tf_op jit(solution)/shard_map/all_gather | solution.py:56
  229.6 5.9 %fusion.55 = f32[256,1408]{1,0:T(8,128)} fusion(bf16[256,2048]{1,0:T(8,128)(2,1)} %all-gather.5.cloned.1.call-done, bf16[2048,1408]{1,0:T(8,128)(2,1)} %all-gather.7.cloned.1.call-done), kind=kOutput, calls=%fused_computation.106 | convolution fusion | flops 1476395008 | bytes 8257536 | tf_op jit(solution)/shard_map/dot_general | solution.py:117
  235.5 87.3 %all-gather.11.cloned.1.call-done = bf16[1408,2048]{1,0:T(8,128)(2,1)} async-done(((bf16[1408,256]{1,0:T(8,128)(2,1)}), bf16[1408,2048]{1,0:T(8,128)(2,1)}) %all-gather.11.cloned.1.call-update) | async-done | bytes 5767184 | tf_op jit(solution)/shard_map/all_gather | solution.py:59
  322.9 92.6 %all-gather.9.cloned.1.call-done = bf16[2048,1408]{1,0:T(8,128)(2,1)} async-done(((bf16[256,1408]{1,0:T(8,128)(2,1)}), bf16[2048,1408]{1,0:T(8,128)(2,1)}) %all-gather.9.cloned.1.call-update) | async-done | bytes 5767184 | tf_op jit(solution)/shard_map/all_gather | solution.py:57
  415.4 9.5 %convolution_convert_fusion.1 = bf16[256,2048]{1,0:T(8,128)(2,1)} fusion(bf16[1408,2048]{1,0:T(8,128)(2,1)} %all-gather.11.cloned.1.call-done, bf16[256,2048]{1,0:T(8,128)(2,1)} %all-gather.5.cloned.1.call-done, bf16[2048,1408]{1,0:T(8,128)(2,1)} %all-gather.9.cloned.1.call-done, f32[256,1408]{1,0:T(8,128)} %fusion.55), kind=kOutput, calls=%fused_computation.10 | convolution fusion | flops 2955476992 | bytes 15073280 | tf_op jit(solution)/shard_map/dot_general | solution.py:120
  425.0 23.2 %reduce-scatter.5.cloned.1.call-done = bf16[64,2048]{1,0:T(8,128)(2,1)} async-done(((bf16[256,2048]{1,0:T(8,128)(2,1)}), bf16[64,2048]{1,0:T(8,128)(2,1)}) %reduce-scatter.5.cloned.1.call-update) | async-done | bytes 262160 | tf_op jit(solution)/shard_map/reduce_scatter | solution.py:121
  448.1 1.8 fusion.22
  (68 shorter events, 13.1 us)
Async XLA Ops:
  6.5 84.7 %copy-start = (bf16[512,2048]{1,0:T(8,128)(2,1)S(1)}, bf16[512,2048]{1,0:T(8,128)(2,1)}, u32[]{:S(2)}) copy-start(bf16[512,2048]{1,0:T(8,128)(2,1)} %param.17) | copy-start | bytes 6291460
  6.5 8.5 %copy-start.6 = (f32[128]{0:T(128)S(1)}, f32[128]{0:T(128)}, u32[]{:S(2)}) copy-start(f32[128]{0:T(128)} %param.16) | copy-start | bytes 1540
  6.5 108.7 %reduce-scatter.3.cloned.1.call-start = ((), (), s32[]{:S(2)}) async-start(), calls=%async_computation.2 | async-start | bytes 1310720 | tf_op jit(solution)/shard_map/reduce_scatter | solution.py:105
  6.5 11.0 %collective-permute-start = (bf16[256,1,128]{2,0,1:T(8,128)(2,1)}, bf16[256,1,128]{2,0,1:T(8,128)(2,1)}, u32[]{:S(2)}, u32[]{:S(2)}) collective-permute-start(bf16[256,1,128]{2,0,1:T(8,128)(2,1)} %bitcast.76), channel_id=1, source_target_pairs={{0,4},{4,8},{8,12},{12,16},{16,20},{20,24},{24,28},{28,0},{1,5},{5... | collective-permute-start | bytes 196616 | tf_op jit(solution)/shard_map/ppermute | solution.py:75
  17.6 7.2 %collective-permute-start.1 = (bf16[256,1,128]{2,0,1:T(8,128)(2,1)}, bf16[256,1,128]{2,0,1:T(8,128)(2,1)S(1)}, u32[]{:S(2)}, u32[]{:S(2)}) collective-permute-start(bf16[256,1,128]{2,0,1:T(8,128)(2,1)} %collective-permute-done), channel_id=1, source_target_pairs={{0,4},{4,8},{8,12},{12,16},{16,20},{20,24},{24,28},{28,0},{1,5},{5... | collective-permute-start | bytes 196616 | tf_op jit(solution)/shard_map/ppermute | solution.py:75
  24.8 7.0 %collective-permute-start.2 = (bf16[256,1,128]{2,0,1:T(8,128)(2,1)S(1)}, bf16[256,1,128]{2,0,1:T(8,128)(2,1)S(1)}, u32[]{:S(2)}, u32[]{:S(2)}) collective-permute-start(bf16[256,1,128]{2,0,1:T(8,128)(2,1)S(1)} %collective-permute-done.1), channel_id=1, source_target_pairs={{0,4},{4,8},{8,12},{12,16},{16,20},{20,24},{24,28},{28,0},{1,5},{5... | collective-permute-start | bytes 196616 | tf_op jit(solution)/shard_map/ppermute | solution.py:75
  31.8 31.5 %collective-permute-start.3 = (bf16[256,1,128]{2,0,1:T(8,128)(2,1)S(1)}, bf16[256,1,128]{2,0,1:T(8,128)(2,1)S(1)}, u32[]{:S(2)}, u32[]{:S(2)}) collective-permute-start(bf16[256,1,128]{2,0,1:T(8,128)(2,1)S(1)} %collective-permute-done.2), channel_id=1, source_target_pairs={{0,4},{4,8},{8,12},{12,16},{16,20},{20,24},{24,28},{28,0},{1,5},{5... | collective-permute-start | bytes 196616 | tf_op jit(solution)/shard_map/ppermute | solution.py:75
  63.3 7.0 %collective-permute-start.4 = (bf16[256,1,128]{2,0,1:T(8,128)(2,1)S(1)}, bf16[256,1,128]{2,0,1:T(8,128)(2,1)S(1)}, u32[]{:S(2)}, u32[]{:S(2)}) collective-permute-start(bf16[256,1,128]{2,0,1:T(8,128)(2,1)S(1)} %collective-permute-done.3), channel_id=1, source_target_pairs={{0,4},{4,8},{8,12},{12,16},{16,20},{20,24},{24,28},{28,0},{1,5},{5... | collective-permute-start | bytes 196616 | tf_op jit(solution)/shard_map/ppermute | solution.py:75
  66.5 3.8 copy-start.1
  66.5 18.6 %copy-start.4 = (bf16[256,128]{1,0:T(8,128)(2,1)S(1)}, bf16[256,128]{1,0:T(8,128)(2,1)}, u32[]{:S(2)}) copy-start(bf16[256,128]{1,0:T(8,128)(2,1)} %param.14) | copy-start | bytes 196612
  70.2 7.0 %collective-permute-start.5 = (bf16[256,1,128]{2,0,1:T(8,128)(2,1)S(1)}, bf16[256,1,128]{2,0,1:T(8,128)(2,1)S(1)}, u32[]{:S(2)}, u32[]{:S(2)}) collective-permute-start(bf16[256,1,128]{2,0,1:T(8,128)(2,1)S(1)} %collective-permute-done.4), channel_id=1, source_target_pairs={{0,4},{4,8},{8,12},{12,16},{16,20},{20,24},{24,28},{28,0},{1,5},{5... | collective-permute-start | bytes 196616 | tf_op jit(solution)/shard_map/ppermute | solution.py:75
  77.2 7.0 %collective-permute-start.6 = (bf16[256,1,128]{2,0,1:T(8,128)(2,1)S(1)}, bf16[256,1,128]{2,0,1:T(8,128)(2,1)S(1)}, u32[]{:S(2)}, u32[]{:S(2)}) collective-permute-start(bf16[256,1,128]{2,0,1:T(8,128)(2,1)S(1)} %collective-permute-done.5), channel_id=1, source_target_pairs={{0,4},{4,8},{8,12},{12,16},{16,20},{20,24},{24,28},{28,0},{1,5},{5... | collective-permute-start | bytes 196616 | tf_op jit(solution)/shard_map/ppermute | solution.py:75
  86.1 29.2 %copy-start.2 = (bf16[64,2048]{1,0:T(8,128)(2,1)S(1)}, bf16[64,2048]{1,0:T(8,128)(2,1)}, u32[]{:S(2)}) copy-start(bf16[64,2048]{1,0:T(8,128)(2,1)} %param.11) | copy-start | bytes 786436
  86.1 30.3 %copy-start.5 = (f32[2048]{0:T(1024)S(1)}, f32[2048]{0:T(1024)}, u32[]{:S(2)}) copy-start(f32[2048]{0:T(1024)} %param.18) | copy-start | bytes 24580
  93.0 42.1 %all-gather.5.cloned.1.call-start = ((), (), s32[]{:S(2)}) async-start(), calls=%async_computation.3 | async-start | bytes 1310720 | tf_op jit(solution)/shard_map/all_gather | solution.py:116
  118.2 111.4 %all-gather.7.cloned.1.call-start = ((), (), s32[]{:S(2)}) async-start(), calls=%async_computation.4 | async-start | bytes 6488064 | tf_op jit(solution)/shard_map/all_gather | solution.py:56
  119.0 203.9 %all-gather.11.cloned.1.call-start = ((), (), s32[]{:S(2)}) async-start(), calls=%async_computation.6 | async-start | bytes 6488064 | tf_op jit(solution)/shard_map/all_gather | solution.py:59
  119.6 295.9 %all-gather.9.cloned.1.call-start = ((), (), s32[]{:S(2)}) async-start(), calls=%async_computation.5 | async-start | bytes 6488064 | tf_op jit(solution)/shard_map/all_gather | solution.py:57
  120.1 328.0 %reduce-scatter.5.cloned.1.call-start = ((), (), s32[]{:S(2)}) async-start(), calls=%async_computation.7 | async-start | bytes 1310720 | tf_op jit(solution)/shard_map/reduce_scatter | solution.py:121
  235.5 212.6 %copy-start.3 = (bf16[64,2048]{1,0:T(8,128)(2,1)S(1)}, bf16[64,2048]{1,0:T(8,128)(2,1)}, u32[]{:S(2)}) copy-start(bf16[64,2048]{1,0:T(8,128)(2,1)} %reduce-scatter.3.cloned.1.call-done) | copy-start | bytes 786436
Sparse Core Ops, SparseCore 0:
  93.2 22.0 reduce-scatter.2
  118.4 16.6 all-gather.4
  137.3 92.2 all-gather.6
  231.5 91.3 all-gather.10
  324.9 90.4 all-gather.8
  425.1 22.9 reduce-scatter.4
